TPU v7x, 32 devices: a whole 2x2x4 slice. The times are simulated.
32 devices in a mesh: rep: 2 (over x), fs: 4 (over z), tp: 4 (over y, core).
Axes of the slice: x: 2, y: 2, z: 4, core: 2. Of those that a mesh axis runs over, the one named last changes fastest.
Arguments:
- tokens: bfloat16 [4096, 2048], P(('rep', 'fs', 'tp')), may hold values from -6 to 6
- norm_gain: float32 [2048], replicated, may hold values from 0.1 to 1.9
- gate_weight: float32 [2048, 5632], P('fs', 'tp'), may hold values from -0.125 to 0.125
- gate_scale: float32 [5632], P('tp'), may hold values from 0.5 to 2
- up_weight: float32 [2048, 5632], P('fs', 'tp'), may hold values from -0.125 to 0.125
- up_scale: float32 [5632], P('tp'), may hold values from 0.5 to 2
- down_weight: float32 [5632, 2048], P('tp', 'fs'), may hold values from -0.078125 to 0.078125
- down_scale: float32 [2048], P('fs'), may hold values from 0.5 to 2
Outputs:
- mixed: bfloat16 [4096, 2048], P(('rep', 'fs', 'tp'))
All inputs are finite; a program needn't handle non-finite values.
Results may differ from a plain program's by a relative error of at most 0.014.
Values may be sent and summed in bfloat16 or wider, within the bound.
No kernel may reach another device: no remote copies, remote signals or barrier semaphores. Data moves between devices by JAX's collectives and lax.ppermute only.
A program may use at most 64 MiB of HBM per device.

v0:
```python
import jax
import jax.numpy as jnp
from jax import lax
from jax.sharding import PartitionSpec as P


def shards(
    tokens, norm_gain, gate_weight, gate_scale, up_weight, up_scale, down_weight, down_scale
):
    flat = tokens.astype(jnp.float32)
    mean_square = jnp.mean(flat * flat, axis=-1, keepdims=True)
    inverse = lax.rsqrt(mean_square + 1e-06)
    normed = (flat * inverse * norm_gain).astype(jnp.bfloat16)
    group = lax.all_gather(normed, "tp", axis=0, tiled=True)
    gate_low = gate_weight.astype(jnp.bfloat16)
    up_low = up_weight.astype(jnp.bfloat16)
    down_low = down_weight.astype(jnp.bfloat16)
    gate = jnp.dot(
        group,
        lax.all_gather(gate_low, "fs", axis=0, tiled=True),
        preferred_element_type=jnp.float32,
    )
    up = jnp.dot(
        group, lax.all_gather(up_low, "fs", axis=0, tiled=True), preferred_element_type=jnp.float32
    )
    down_full = lax.all_gather(down_low, "fs", axis=1, tiled=True)
    gate = gate * gate_scale
    up = up * up_scale
    hidden = (jax.nn.silu(gate) * up).astype(jnp.bfloat16)
    scales = lax.all_gather(down_scale, "fs", axis=0, tiled=True)
    total = lax.psum_scatter(
        jnp.dot(hidden, down_full, preferred_element_type=jnp.float32).astype(jnp.bfloat16),
        "tp",
        scatter_dimension=0,
        tiled=True,
    ).astype(jnp.float32)
    return (total * scales).astype(jnp.bfloat16)


def solution(mesh):
    in_specs = (
        P(("rep", "fs", "tp"), None),
        P(),
        P("fs", "tp"),
        P("tp"),
        P("fs", "tp"),
        P("tp"),
        P("tp", "fs"),
        P("fs"),
    )
    out_specs = P(("rep", "fs", "tp"), None)
    return jax.shard_map(shards, mesh=mesh, in_specs=in_specs, out_specs=out_specs, check_vma=False)
```

profile of v0, /device:TPU:0, one launch (start us, length us, event | category | flops | bytes accessed | tf_op | source)
XLA Modules:
  0.0 408.0 jit_solution(18322760977833249545)
XLA Ops:
  6.5 1.2 fusion.2
  7.8 2.0 fusion.4
  9.8 0.0 all-gather.6.cloned.1.call-update
  9.8 0.0 all-gather.8.cloned.1.call-start
  9.9 3.3 convert_element_type.29
  13.2 0.0 all-gather.8.cloned.1.call-update
  13.2 0.0 all-gather.10.cloned.1.call-start
  13.2 1.3 convert_element_type.30
  14.5 0.0 all-gather.10.cloned.1.call-update
  14.5 0.0 copy-start.3
  14.6 0.0 all-gather.12.cloned.1.call-start
  14.6 3.1 convert_element_type.32
  17.8 0.0 all-gather.12.cloned.1.call-update
  17.8 0.0 reduce-scatter.2.cloned.1.call-start
  17.8 17.4 %all-gather.6.cloned.1.call-done = bf16[512,2048]{1,0:T(8,128)(2,1)} async-done(((bf16[128,2048]{1,0:T(8,128)(2,1)}), bf16[512,2048]{1,0:T(8,128)(2,1)}) %all-gather.6.cloned.1.call-update) | async-done | bytes 2097168 | tf_op jit(solution)/shard_map/all_gather | solution.py:14
  35.3 108.3 %all-gather.8.cloned.1.call-done = bf16[2048,1408]{1,0:T(8,128)(2,1)} async-done(((bf16[512,1408]{1,0:T(8,128)(2,1)}), bf16[2048,1408]{1,0:T(8,128)(2,1)}) %all-gather.8.cloned.1.call-update) | async-done | bytes 5767184 | tf_op jit(solution)/shard_map/all_gather | solution.py:20
  143.6 8.2 %convolution_multiply_fusion.1 = f32[512,1408]{1,0:T(8,128)} fusion(bf16[512,2048]{1,0:T(8,128)(2,1)} %all-gather.6.cloned.1.call-done, bf16[2048,1408]{1,0:T(8,128)(2,1)} %all-gather.8.cloned.1.call-done, f32[1408]{0:T(1024)S(1)} %copy-done.3), kind=kOutput, calls=%fused_computation.2 | convolution fusion | flops 2953510912 | bytes 10753536 | tf_op jit(solution)/shard_map/dot_general | solution.py:18
  151.8 98.3 %all-gather.10.cloned.1.call-done = bf16[2048,1408]{1,0:T(8,128)(2,1)} async-done(((bf16[512,1408]{1,0:T(8,128)(2,1)}), bf16[2048,1408]{1,0:T(8,128)(2,1)}) %all-gather.10.cloned.1.call-update) | async-done | bytes 5767184 | tf_op jit(solution)/shard_map/all_gather | solution.py:24
  250.1 106.4 %all-gather.12.cloned.1.call-done = bf16[1408,2048]{1,0:T(8,128)(2,1)} async-done(((bf16[1408,512]{1,0:T(8,128)(2,1)}), bf16[1408,2048]{1,0:T(8,128)(2,1)}) %all-gather.12.cloned.1.call-update) | async-done | bytes 5767184 | tf_op jit(solution)/shard_map/all_gather | solution.py:26
  356.5 13.4 %convolution_convert_fusion = bf16[512,2048]{1,0:T(8,128)(2,1)} fusion(bf16[1408,2048]{1,0:T(8,128)(2,1)} %all-gather.12.cloned.1.call-done, bf16[512,2048]{1,0:T(8,128)(2,1)S(1)} %copy-done.2, bf16[2048,1408]{1,0:T(8,128)(2,1)} %all-gather.10.cloned.1.call-done, f32[512,1408]{1,0:T(8,128)} %convolution_multiply_fusion.1, f32[1408]{0:T(1024)S(1)} %copy-done.4), kind=kOutput, calls=%fused_computation.4 | convolution fusion | flops 5911674880 | bytes 18617856 | tf_op jit(solution)/shard_map/dot_general | solution.py:32
  370.0 0.0 reduce-scatter.2.cloned.1.call-update
  370.0 11.9 %all-gather = f32[4,1,512]{2,1,0:T(1,128)S(1)} all-gather(f32[1,1,512]{2,1,0:T(1,128)S(1)} %bitcast.8), channel_id=1, replica_groups=mesh['rep'=2,'fs'=4,'tp'=4] {'fs'}, dimensions={0}, use_global_device_ids=true | all-gather | bytes 10240 | tf_op jit(solution)/shard_map/all_gather | solution.py:30
  381.9 17.6 %reduce-scatter.2.cloned.1.call-done = bf16[128,2048]{1,0:T(8,128)(2,1)} async-done(((bf16[512,2048]{1,0:T(8,128)(2,1)}), bf16[128,2048]{1,0:T(8,128)(2,1)}) %reduce-scatter.2.cloned.1.call-update) | async-done | bytes 524304 | tf_op jit(solution)/shard_map/reduce_scatter | solution.py:31
  399.6 1.9 multiply_convert_fusion
  (11 shorter events, 0.0 us)
Async XLA Ops:
  6.5 28.7 %all-gather.6.cloned.1.call-start = ((), (), s32[]{:S(2)}) async-start(), calls=%async_computation.1 | async-start | bytes 2621440 | tf_op jit(solution)/shard_map/all_gather | solution.py:14
  9.8 3.4 copy-start
  9.8 133.7 %all-gather.8.cloned.1.call-start = ((), (), s32[]{:S(2)}) async-start(), calls=%async_computation.2 | async-start | bytes 7208960 | tf_op jit(solution)/shard_map/all_gather | solution.py:20
  13.2 236.9 %all-gather.10.cloned.1.call-start = ((), (), s32[]{:S(2)}) async-start(), calls=%async_computation.3 | async-start | bytes 7208960 | tf_op jit(solution)/shard_map/all_gather | solution.py:24
  14.5 129.0 %copy-start.3 = (f32[1408]{0:T(1024)S(1)}, f32[1408]{0:T(1024)}, u32[]{:S(2)}) copy-start(f32[1408]{0:T(1024)} %param.11) | copy-start | bytes 16900
  14.6 342.0 %all-gather.12.cloned.1.call-start = ((), (), s32[]{:S(2)}) async-start(), calls=%async_computation.4 | async-start | bytes 7208960 | tf_op jit(solution)/shard_map/all_gather | solution.py:26
  17.8 338.7 %copy-start.4 = (f32[1408]{0:T(1024)S(1)}, f32[1408]{0:T(1024)}, u32[]{:S(2)}) copy-start(f32[1408]{0:T(1024)} %param.13) | copy-start | bytes 16900
  17.8 381.8 %reduce-scatter.2.cloned.1.call-start = ((), (), s32[]{:S(2)}) async-start(), calls=%async_computation.5 | async-start | bytes 2621440 | tf_op jit(solution)/shard_map/reduce_scatter | solution.py:31
  35.3 321.2 %copy-start.2 = (bf16[512,2048]{1,0:T(8,128)(2,1)S(1)}, bf16[512,2048]{1,0:T(8,128)(2,1)}, u32[]{:S(2)}) copy-start(bf16[512,2048]{1,0:T(8,128)(2,1)} %all-gather.6.cloned.1.call-done) | copy-start | bytes 6291460
  151.8 218.2 %copy-start.1 = (f32[512]{0:T(512)S(1)}, f32[512]{0:T(512)}, u32[]{:S(2)}) copy-start(f32[512]{0:T(512)} %param.15) | copy-start | bytes 6148
Sparse Core Ops, SparseCore 0:
  9.9 25.2 all-gather.5
  36.8 106.6 all-gather.7
  145.1 104.9 all-gather.9
  251.5 104.9 all-gather.11
  370.1 29.4 reduce-scatter.1
where the time goes:
time: 408 us
  waiting for transfers between devices  348 us (85%)
  matrix products  21.7 us (5%)
  between operations  13.2 us (3%)
  other arithmetic  12.9 us (3%)
  blocking collectives  11.9 us (3%)
    all_gather x1, waiting for transfers between devices, shards(): lax.all_gather(gate_low, 'fs', axis=0, tiled=True)  108 us
    all_gather x1, waiting for transfers between devices, shards(): down_full = lax.all_gather(down_low, 'fs', axis=1, tiled=True)  106 us
    all_gather x1, waiting for transfers between devices, shards(): lax.all_gather(up_low, 'fs', axis=0, tiled=True)  98.3 us
    reduce_scatter x1, waiting for transfers between devices, shards(): lax.psum_scatter(jnp.dot(hidden, down_full, preferred_element_type=jnp.fl...  17.6 us
    all_gather x1, waiting for transfers between devices, shards(): group = lax.all_gather(normed, 'tp', axis=0, tiled=True)  17.4 us
    dot_general x1, matrix products, shards(): jnp.dot(hidden, down_full, preferred_element_type=jnp.float32)  13.4 us
    all_gather x1, blocking collectives, shards(): scales = lax.all_gather(down_scale, 'fs', axis=0, tiled=True)  11.9 us
    dot_general x1, matrix products, shards(): jnp.dot(group, lax.all_gather(gate_low, 'fs', axis=0, tiled=True), prefer...  8.23 us
  transfers between devices with their start and end apart: 5, of which 5 were waited for; matrix products, arithmetic and copies ran while one was open for 4% of the time, Pallas kernels for 0%

commit v1 on v0

--- a/solution.py
+++ b/solution.py
@@ -2,6 +2,15 @@
 import jax.numpy as jnp
 from jax import lax
 from jax.sharding import PartitionSpec as P
+
+
+def treat_the_set(shard_axis, matrix):
+    return jnp.concatenate(
+        lax.all_to_all(
+            jnp.stack(lax.axis_size(shard_axis) * [matrix]), shard_axis, split_axis=0, concat_axis=0
+        ),
+        axis=1,
+    )
 
 
 def shards(
@@ -23,7 +32,7 @@
     up = jnp.dot(
         group, lax.all_gather(up_low, "fs", axis=0, tiled=True), preferred_element_type=jnp.float32
     )
-    down_full = lax.all_gather(down_low, "fs", axis=1, tiled=True)
+    down_full = treat_the_set("fs", down_low)
     gate = gate * gate_scale
     up = up * up_scale
     hidden = (jax.nn.silu(gate) * up).astype(jnp.bfloat16)

time: 408 us -> 405 us (level)
  waiting for transfers between devices: 348 us -> 336 us
  starting transfers between devices: 0.17 us -> 6.7 us
    all_gather x1 -> x0, waiting for transfers between devices: 106 us -> none  [shards(): down_full = lax.all_gather(down_low, 'fs', axis=1, tiled=True)]
    all_gather x1, waiting for transfers between devices: 108 us -> 196 us  [shards(): lax.all_gather(gate_low, 'fs', axis=0, tiled=True)]
    all_gather x1, waiting for transfers between devices: 98.3 us -> 108 us  [shards(): lax.all_gather(up_low, 'fs', axis=0, tiled=True)]
    all_gather x1, waiting for transfers between devices: 17.4 us -> 8.6 us  [shards(): group = lax.all_gather(normed, 'tp', axis=0, tiled=True)]
    all_to_all x0 -> x1, starting transfers between devices: none -> 6.61 us  [treat_the_set(): lax.all_to_all(jnp.stack(lax.axis_size(shard_axis) * [matrix]), shard_axi...]
    all_to_all x0 -> x1, waiting for transfers between devices: none -> 5.79 us  [treat_the_set(): lax.all_to_all(jnp.stack(lax.axis_size(shard_axis) * [matrix]), shard_axi...]
  transfers between devices with their start and end apart: 5 -> 5, of which waited for: 5 -> 5; matrix products, arithmetic and copies ran while one was open for 4% -> 5% of each run, Pallas kernels for 0% -> 0%
where the time goes in v1:
time: 405 us
  waiting for transfers between devices  336 us (83%)
  matrix products  21.7 us (5%)
  between operations  13.2 us (3%)
  blocking collectives  11.9 us (3%)
  other arithmetic  11.5 us (3%)
  starting transfers between devices  6.7 us (2%)
    all_gather x1, waiting for transfers between devices, shards(): lax.all_gather(gate_low, 'fs', axis=0, tiled=True)  196 us
    all_gather x1, waiting for transfers between devices, shards(): lax.all_gather(up_low, 'fs', axis=0, tiled=True)  108 us
    reduce_scatter x1, waiting for transfers between devices, shards(): lax.psum_scatter(jnp.dot(hidden, down_full, preferred_element_type=jnp.fl...  17.6 us
    dot_general x1, matrix products, shards(): jnp.dot(hidden, down_full, preferred_element_type=jnp.float32)  13.4 us
    all_gather x1, blocking collectives, shards(): scales = lax.all_gather(down_scale, 'fs', axis=0, tiled=True)  11.9 us
    all_gather x1, waiting for transfers between devices, shards(): group = lax.all_gather(normed, 'tp', axis=0, tiled=True)  8.6 us
    dot_general x1, matrix products, shards(): jnp.dot(group, lax.all_gather(gate_low, 'fs', axis=0, tiled=True), prefer...  8.3 us
  transfers between devices with their start and end apart: 5, of which 5 were waited for; matrix products, arithmetic and copies ran while one was open for 5% of the time, Pallas kernels for 0%

profile of v1, /device:TPU:0, one launch (start us, length us, event | category | flops | bytes accessed | tf_op | source)
XLA Modules:
  0.0 404.6 jit_solution(12974803916923759330)
XLA Ops:
  6.5 1.2 fusion.2
  7.8 2.0 fusion.4
  9.8 0.0 all-gather.5.cloned.1.call-update
  9.8 0.0 all-gather.7.cloned.1.call-start
  9.9 3.1 convert_element_type.29
  12.9 0.0 all-gather.7.cloned.1.call-update
  13.0 2.0 convert_element_type.32
  15.0 0.8 copy.10
  15.8 2.9 stack.2
  18.7 6.6 %all-to-all-start = ((bf16[4,1408,512]{1,2,0:T(8,128)(2,1)}), bf16[4,1408,512]{1,2,0:T(8,128)(2,1)}, u32[]{:S(2)}, u32[]{:S(2)}) async-start(bf16[4,1408,512]{1,2,0:T(8,128)(2,1)} %stack.2), calls=%async_computation | async-start | bytes 11534336 | tf_op jit(solution)/shard_map/all_to_all | solution.py:9
  25.3 1.3 convert_element_type.30
  26.6 0.0 all-gather.9.cloned.1.call-update
  26.6 0.0 copy-start.4
  26.6 0.0 reduce-scatter.2.cloned.1.call-start
  26.7 8.6 %all-gather.5.cloned.1.call-done = bf16[512,2048]{1,0:T(8,128)(2,1)} async-done(((bf16[128,2048]{1,0:T(8,128)(2,1)}), bf16[512,2048]{1,0:T(8,128)(2,1)}) %all-gather.5.cloned.1.call-update) | async-done | bytes 2097168 | tf_op jit(solution)/shard_map/all_gather | solution.py:23
  35.3 196.1 %all-gather.7.cloned.1.call-done = bf16[2048,1408]{1,0:T(8,128)(2,1)} async-done(((bf16[512,1408]{1,0:T(8,128)(2,1)}), bf16[2048,1408]{1,0:T(8,128)(2,1)}) %all-gather.7.cloned.1.call-update) | async-done | bytes 5767184 | tf_op jit(solution)/shard_map/all_gather | solution.py:29
  231.3 8.3 %convolution_multiply_fusion.1 = f32[512,1408]{1,0:T(8,128)} fusion(bf16[512,2048]{1,0:T(8,128)(2,1)} %all-gather.5.cloned.1.call-done, bf16[2048,1408]{1,0:T(8,128)(2,1)} %all-gather.7.cloned.1.call-done, f32[1408]{0:T(1024)S(1)} %copy-done.3), kind=kOutput, calls=%fused_computation.2 | convolution fusion | flops 2953510912 | bytes 10753536 | tf_op jit(solution)/shard_map/dot_general | solution.py:27
  239.6 5.8 %all-to-all-done = bf16[4,1408,512]{1,2,0:T(8,128)(2,1)} async-done(((bf16[4,1408,512]{1,2,0:T(8,128)(2,1)}), bf16[4,1408,512]{1,2,0:T(8,128)(2,1)}, u32[]{:S(2)}, u32[]{:S(2)}) %all-to-all-start) | async-done | bytes 5767200 | tf_op jit(solution)/shard_map/all_to_all | solution.py:9
  245.4 107.7 %all-gather.9.cloned.1.call-done = bf16[2048,1408]{1,0:T(8,128)(2,1)} async-done(((bf16[512,1408]{1,0:T(8,128)(2,1)}), bf16[2048,1408]{1,0:T(8,128)(2,1)}) %all-gather.9.cloned.1.call-update) | async-done | bytes 5767184 | tf_op jit(solution)/shard_map/all_gather | solution.py:33
  353.1 13.4 %convolution_convert_fusion = bf16[512,2048]{1,0:T(8,128)(2,1)} fusion(bf16[1408,2048]{0,1:T(8,128)(2,1)} %bitcast.1, bf16[512,2048]{1,0:T(8,128)(2,1)S(1)} %copy-done.2, bf16[2048,1408]{1,0:T(8,128)(2,1)} %all-gather.9.cloned.1.call-done, f32[512,1408]{1,0:T(8,128)} %convolution_multiply_fusion.1, f32[1408]{0:T(1024)S(1)} %copy-done.4), kind=kOutput, calls=%fused_computation.4 | convolution fusion | flops 5911674880 | bytes 18617856 | tf_op jit(solution)/shard_map/dot_general | solution.py:41
  366.5 0.0 reduce-scatter.2.cloned.1.call-update
  366.6 11.9 %all-gather = f32[4,1,512]{2,1,0:T(1,128)S(1)} all-gather(f32[1,1,512]{2,1,0:T(1,128)S(1)} %bitcast.11), channel_id=1, replica_groups=mesh['rep'=2,'fs'=4,'tp'=4] {'fs'}, dimensions={0}, use_global_device_ids=true | all-gather | bytes 10240 | tf_op jit(solution)/shard_map/all_gather | solution.py:39
  378.5 17.6 %reduce-scatter.2.cloned.1.call-done = bf16[128,2048]{1,0:T(8,128)(2,1)} async-done(((bf16[512,2048]{1,0:T(8,128)(2,1)}), bf16[128,2048]{1,0:T(8,128)(2,1)}) %reduce-scatter.2.cloned.1.call-update) | async-done | bytes 524304 | tf_op jit(solution)/shard_map/reduce_scatter | solution.py:40
  396.2 1.9 multiply_convert_fusion
  (12 shorter events, 0.0 us)
Async XLA Ops:
  6.5 28.7 %all-gather.5.cloned.1.call-start = ((), (), s32[]{:S(2)}) async-start(), calls=%async_computation.2 | async-start | bytes 2621440 | tf_op jit(solution)/shard_map/all_gather | solution.py:23
  9.8 221.5 %all-gather.7.cloned.1.call-start = ((), (), s32[]{:S(2)}) async-start(), calls=%async_computation.3 | async-start | bytes 7208960 | tf_op jit(solution)/shard_map/all_gather | solution.py:29
  18.7 6.6 %copy-start = (f32[512,1408]{1,0:T(8,128)S(1)}, f32[512,1408]{1,0:T(8,128)}, u32[]{:S(2)}) copy-start(f32[512,1408]{1,0:T(8,128)} %param.12) | copy-start | bytes 8650756
  18.7 226.7 %all-to-all-start = ((bf16[4,1408,512]{1,2,0:T(8,128)(2,1)}), bf16[4,1408,512]{1,2,0:T(8,128)(2,1)}, u32[]{:S(2)}, u32[]{:S(2)}) async-start(bf16[4,1408,512]{1,2,0:T(8,128)(2,1)} %stack.2), calls=%async_computation | async-start | bytes 11534336 | tf_op jit(solution)/shard_map/all_to_all | solution.py:9
  25.3 206.0 %copy-start.3 = (f32[1408]{0:T(1024)S(1)}, f32[1408]{0:T(1024)}, u32[]{:S(2)}) copy-start(f32[1408]{0:T(1024)} %param.11) | copy-start | bytes 16900
  25.3 327.8 %all-gather.9.cloned.1.call-start = ((), (), s32[]{:S(2)}) async-start(), calls=%async_computation.4 | async-start | bytes 7208960 | tf_op jit(solution)/shard_map/all_gather | solution.py:33
  26.6 326.5 %copy-start.4 = (f32[1408]{0:T(1024)S(1)}, f32[1408]{0:T(1024)}, u32[]{:S(2)}) copy-start(f32[1408]{0:T(1024)} %param.13) | copy-start | bytes 16900
  26.6 369.5 %reduce-scatter.2.cloned.1.call-start = ((), (), s32[]{:S(2)}) async-start(), calls=%async_computation.5 | async-start | bytes 2621440 | tf_op jit(solution)/shard_map/reduce_scatter | solution.py:40
  35.3 317.8 %copy-start.2 = (bf16[512,2048]{1,0:T(8,128)(2,1)S(1)}, bf16[512,2048]{1,0:T(8,128)(2,1)}, u32[]{:S(2)}) copy-start(bf16[512,2048]{1,0:T(8,128)(2,1)} %all-gather.5.cloned.1.call-done) | copy-start | bytes 6291460
  353.1 13.4 %copy-start.1 = (f32[512]{0:T(512)S(1)}, f32[512]{0:T(512)}, u32[]{:S(2)}) copy-start(f32[512]{0:T(512)} %param.15) | copy-start | bytes 6148
Sparse Core Ops, SparseCore 0:
  9.9 25.2 all-gather.4
  36.8 194.4 all-gather.6
  232.9 120.1 all-gather.8
  366.7 29.4 reduce-scatter.1
